TPU v7x, 32 devices: a whole 2x2x4 slice. The times are simulated.
32 devices in a mesh: kv: 4 (over y, x), tp: 8 (over z, core).
Axes of the slice: x: 2, y: 2, z: 4, core: 2. Of those that a mesh axis runs over, the one named last changes fastest.
Arguments:
- tokens: bfloat16 [512, 2048], P('tp', 'kv'), may hold values from -16 to 16
- lengths: int32 [512], P('tp'), may hold values from 1 to 8192, 524288 in all
- query_weight: bfloat16 [2048, 1024], P(None, 'kv'), may hold values from -0.125 to 0.125
- key_weight: bfloat16 [2048, 1024], P(None, 'kv'), may hold values from -0.125 to 0.125
- value_weight: bfloat16 [2048, 1024], P(None, 'kv'), may hold values from -0.125 to 0.125
- gate_weight: bfloat16 [2048, 1024], P(None, 'kv'), may hold values from -0.125 to 0.125
- output_weight: bfloat16 [1024, 2048], P('kv'), may hold values from -0.1875 to 0.1875
- mixer_gain: float32 [2048], replicated, may hold values from 0.1 to 1.9
- group_gain: float32 [1024], P('kv'), may hold values from 0.1 to 1.9
- channel_gain: float32 [2048], P('kv'), may hold values from 0.1 to 1.9
- up_weight: bfloat16 [2048, 8192], P('kv', 'tp'), may hold values from -0.125 to 0.125
- down_weight: bfloat16 [8192, 2048], P('tp', 'kv'), may hold values from -0.0625 to 0.0625
- memory_state: float32 [512, 16, 64, 64], P('tp', 'kv'), may hold values from -0.6 to 0.6
Outputs:
- mixed: bfloat16 [512, 2048], P('tp', 'kv')
- new_state: float32 [512, 16, 64, 64], P('tp', 'kv')
All inputs are finite; a program needn't handle non-finite values. No bound on the sum of `lengths` on one device may be relied on, other than what follows from the above.
Results may differ from a plain program's by a relative error of at most 0.012.
Values may be sent and summed in bfloat16 or wider, within the bound.
A program may use at most 64 MiB of HBM per device.

v0:
```python
import jax
import jax.numpy as jnp
from jax import lax
from jax.sharding import PartitionSpec as P

D = 2048
HEADS = 16
HEAD_DIM = 64


EPS = 1e-06
THETA = 10000.0


def rotate(vectors, position):
    breadth = vectors.shape[-1]
    middle = breadth // 2
    inverse = THETA ** (-jnp.arange(middle, dtype=jnp.float32) * 2.0 / breadth)
    angles = position.astype(jnp.float32)[:, None] * inverse[None, :]
    cosine = jnp.cos(angles)[:, None, :]
    sine_part = jnp.sin(angles)[:, None, :]
    former = vectors[..., :middle]
    latter = vectors[..., middle:]
    return jnp.concatenate(
        [former * cosine - latter * sine_part, former * sine_part + latter * cosine], axis=-1
    )


def on_device(
    tokens,
    lengths,
    query_weight,
    key_weight,
    value_weight,
    gate_weight,
    output_weight,
    mixer_gain,
    group_gain,
    channel_gain,
    up_weight,
    down_weight,
    memory_state,
):
    whole_rows = lax.all_gather(tokens, "kv", axis=1, tiled=True)
    widened = whole_rows.astype(jnp.float32)
    normed = (
        widened * lax.rsqrt(jnp.mean(widened * widened, axis=1, keepdims=True) + EPS) * mixer_gain
    ).astype(jnp.bfloat16)
    served = tokens.shape[0]
    local_heads = query_weight.shape[1] // HEAD_DIM

    def project(weight):
        return jnp.dot(normed, weight, preferred_element_type=jnp.float32).reshape(
            served, local_heads, HEAD_DIM
        )

    queries = rotate(project(query_weight), lengths)
    keys_new = rotate(project(key_weight), lengths) * HEAD_DIM ** (-0.5)
    values_new = project(value_weight)
    gating = jnp.dot(normed, gate_weight, preferred_element_type=jnp.float32)
    head_ids = (lax.axis_index("kv") * local_heads + jnp.arange(local_heads)).astype(jnp.float32)
    decays = 1.0 - 2.0 ** (-5.0 - 5.0 * head_ids / (HEADS - 1))
    new_state = (
        decays[None, :, None, None] * memory_state
        + keys_new[:, :, :, None] * values_new[:, :, None, :]
    )
    readout = jnp.einsum("bhkv,bhk->bhv", new_state, queries, precision=lax.Precision.HIGHEST)
    grouped = readout * lax.rsqrt(jnp.mean(readout * readout, axis=-1, keepdims=True) + EPS)
    grouped = grouped * group_gain.reshape(local_heads, HEAD_DIM)
    merged = (grouped.reshape(served, local_heads * HEAD_DIM) * jax.nn.silu(gating)).astype(
        jnp.bfloat16
    )
    partial_value = jnp.dot(merged, output_weight, preferred_element_type=jnp.float32)
    mixed_part = lax.psum_scatter(partial_value, "kv", scatter_dimension=1, tiled=True)
    after_mixer = (tokens.astype(jnp.float32) + mixed_part).astype(jnp.bfloat16)
    all_rows = lax.all_gather(after_mixer, "tp", axis=0, tiled=True)
    residual = all_rows.astype(jnp.float32)
    squares = jnp.sum(residual * residual, axis=1)
    scaled = (residual * channel_gain).astype(jnp.bfloat16)
    raised_part = jnp.dot(scaled, up_weight, preferred_element_type=jnp.float32)
    raised, totals = (
        lax.psum_scatter(raised_part, "kv", scatter_dimension=0, tiled=True),
        lax.psum_scatter(squares, "kv", scatter_dimension=0, tiled=True),
    )
    factor = lax.rsqrt(totals / D + EPS)
    shared = jnp.square(jax.nn.relu(raised * factor[:, None])).astype(jnp.bfloat16)
    hidden = lax.all_gather(shared, "kv", axis=0, tiled=True)
    lowered = lax.psum_scatter(
        jnp.dot(hidden, down_weight, preferred_element_type=jnp.float32),
        "tp",
        scatter_dimension=0,
        tiled=True,
    )
    mixed = (after_mixer.astype(jnp.float32) + lowered).astype(jnp.bfloat16)
    return (mixed, new_state)


def solution(mesh):
    return jax.shard_map(
        on_device,
        mesh=mesh,
        in_specs=(
            P("tp", "kv"),
            P("tp"),
            P(None, "kv"),
            P(None, "kv"),
            P(None, "kv"),
            P(None, "kv"),
            P("kv", None),
            P(),
            P("kv"),
            P("kv"),
            P("kv", "tp"),
            P("tp", "kv"),
            P("tp", "kv", None, None),
        ),
        out_specs=(P("tp", "kv"), P("tp", "kv", None, None)),
        check_vma=False,
    )
```

profile of v0, /device:TPU:0, one launch (start us, length us, event | category | flops | bytes accessed | tf_op | source)
XLA Modules:
  0.0 197.3 jit_solution(14836653265348833495)
XLA Ops:
  7.2 0.0 copy-start
  7.2 0.0 reduce-scatter.4.cloned.1.call-start
  7.3 0.7 convert_element_type.45
  8.0 0.8 mul.216
  8.8 10.7 %all_gather.9 = bf16[64,2048]{1,0:T(8,128)(2,1)S(1)} all-gather(bf16[64,512]{1,0:T(8,128)(2,1)} %param.13), channel_id=1, replica_groups=mesh['kv'=4,'tp'=8] {'kv'}, dimensions={1}, use_global_device_ids=true | all-gather | bytes 327680 | tf_op jit(solution)/shard_map/all_gather | solution.py:44
  19.5 0.2 fusion.2
  19.7 1.6 fusion.17
  21.2 0.1 mul.206
  21.4 1.6 fusion.15
  23.0 0.1 reshape.110
  23.1 1.6 fusion.19
  24.7 0.1 reshape.109
  24.8 0.2 multiply_cosine_fusion
  25.0 0.3 multiply_subtract_fusion
  25.3 0.2 maximum_multiply_fusion
  25.5 5.4 %multiply_add_fusion = f32[64,4,64,64]{3,2,1,0:T(8,128)S(1)} fusion(f32[64,4,64,64]{3,2,1,0:T(8,128)} %param.25, f32[64,4,64]{2,1,0:T(4,128)S(1)} %mul.206, f32[64,4,64]{2,1,0:T(4,128)S(1)} %get-tuple-element.10, f32[4]{0:T(128)S(1)} %power_subtract_fusion), kind=kLoop, calls=%fused_computation | loop fusion | flops 3145728 | bytes 8519696 | tf_op jit(solution)/shard_map/add | solution.py:64
  30.8 0.0 copy-start.1
  30.8 0.0 copy-start.2
  30.9 0.0 copy-start.3
  30.9 0.0 copy-start.4
  30.9 3.5 %copy-done.1 = f32[64,4,64,64]{3,2,1,0:T(8,128)} copy-done((f32[64,4,64,64]{3,2,1,0:T(8,128)}, f32[64,4,64,64]{3,2,1,0:T(8,128)S(1)}, u32[]{:S(2)}) %copy-start.1) | copy-done | bytes 4194328
  34.4 7.3 %fusion.25 = f32[64,4,1,64]{3,2,1,0:T(1,128)S(1)} fusion(f32[64,4,64,64]{3,2,1,0:T(8,128)S(1)} %multiply_add_fusion, f32[64,4,64,1]{2,3,1,0:T(1,128)S(1)} %bitcast.18), kind=kOutput, calls=%fused_computation.40 | convolution fusion | flops 12582912 | bytes 4325376 | tf_op jit(solution)/shard_map/bhkv,bhk->bhv/dot_general | solution.py:67
  41.7 0.1 multiply_reduce_fusion
  41.9 0.1 multiply_multiply_fusion
  42.0 0.8 reshape.111
  42.8 0.0 copy-done.2
  42.8 0.0 copy-done.3
  42.8 0.0 copy-done.4
  42.8 2.5 %fusion.8 = f32[64,2048]{1,0:T(8,128)} fusion(bf16[256,2048]{1,0:T(8,128)(2,1)S(1)} %copy-done.2, f32[64,256]{1,0:T(8,128)} %reshape.111, bf16[2048,256]{1,0:T(8,128)(2,1)S(1)} %copy-done.3, bf16[64,2048]{1,0:T(8,128)(2,1)S(1)} %all_gather.9, f32[2048]{0:T(1024)S(1)} %copy-done.4, f32[64]{0:T(128)S(1)} %add_rsqrt_fusion.1), kind=kOutput, calls=%fused_computation.26 | convolution fusion | flops 134840320 | bytes 2957568 | tf_op jit(solution)/shard_map/dot_general | solution.py:73
  45.3 0.0 copy-start.5
  45.3 0.0 reduce-scatter.4.cloned.1.call-update
  45.3 0.0 reduce-scatter.6.cloned.1.call-start
  45.4 25.5 %reduce-scatter.4.cloned.1.call-done = f32[64,512]{1,0:T(8,128)} async-done(((f32[64,2048]{1,0:T(8,128)}), f32[64,512]{1,0:T(8,128)}) %reduce-scatter.4.cloned.1.call-update) | async-done | bytes 131088 | tf_op jit(solution)/shard_map/reduce_scatter | solution.py:74
  70.8 0.9 add_convert_fusion.1
  71.7 14.7 %all_gather.10 = bf16[512,512]{1,0:T(8,128)(2,1)S(1)} all-gather(bf16[64,512]{1,0:T(8,128)(2,1)S(1)} %add_convert_fusion.1), channel_id=1, replica_groups=mesh['kv'=4,'tp'=8] {'tp'}, dimensions={0}, use_global_device_ids=true | all-gather | bytes 589824 | tf_op jit(solution)/shard_map/all_gather | solution.py:76
  86.5 0.0 copy-done
  86.5 2.7 %fusion.5 = f32[512,1024]{1,0:T(8,128)} fusion(bf16[512,1024]{1,0:T(8,128)(2,1)S(1)} %copy-done, bf16[512,512]{1,0:T(8,128)(2,1)S(1)} %all_gather.10, f32[512]{0:T(512)} %param.22), kind=kOutput, calls=%fused_computation.10 | convolution fusion | flops 537657344 | bytes 3672064 | tf_op jit(solution)/shard_map/dot_general | solution.py:80
  89.2 0.0 reduce-scatter.6.cloned.1.call-update
  89.3 0.0 all-gather.2.cloned.1.call-start
  89.3 1.2 dynamic-slice
  91.2 0.2 fusion.1
  91.4 9.0 %all-reduce = f32[512]{0:T(512)S(1)} all-reduce(f32[512]{0:T(512)S(1)} %fusion.1), channel_id=4, replica_groups=mesh['kv'=4,'tp'=8] {'kv'}, use_global_device_ids=true, to_apply=%region_5.6.clone | all-reduce | flops 512 | bytes 4096
  100.4 0.1 fusion.11
  100.5 24.3 %reduce-scatter.6.cloned.1.call-done = f32[128,1024]{1,0:T(8,128)} async-done(((f32[512,1024]{1,0:T(8,128)}), f32[128,1024]{1,0:T(8,128)}) %reduce-scatter.6.cloned.1.call-update) | async-done | bytes 524304 | tf_op jit(solution)/shard_map/reduce_scatter | solution.py:82
  124.8 1.9 multiply_convert_fusion
  126.7 0.0 all-gather.2.cloned.1.call-update
  126.7 0.0 reduce-scatter.8.cloned.1.call-start
  126.7 26.6 %all-gather.2.cloned.1.call-done = bf16[512,1024]{1,0:T(8,128)(2,1)} async-done(((bf16[128,1024]{1,0:T(8,128)(2,1)}), bf16[512,1024]{1,0:T(8,128)(2,1)}) %all-gather.2.cloned.1.call-update) | async-done | bytes 1048592 | tf_op jit(solution)/shard_map/all_gather | solution.py:87
  153.3 0.0 copy-done.5
  153.3 3.0 %fusion.26 = f32[512,512]{1,0:T(8,128)} fusion(bf16[512,1024]{1,0:T(8,128)(2,1)} %all-gather.2.cloned.1.call-done, bf16[1024,512]{1,0:T(8,128)(2,1)S(1)} %copy-done.5), kind=kOutput, calls=%fused_computation.41 | convolution fusion | flops 536870912 | bytes 3145728 | tf_op jit(solution)/shard_map/dot_general | solution.py:89
  156.3 0.0 reduce-scatter.8.cloned.1.call-update
  156.3 32.8 %reduce-scatter.8.cloned.1.call-done = f32[64,512]{1,0:T(8,128)} async-done(((f32[512,512]{1,0:T(8,128)}), f32[64,512]{1,0:T(8,128)}) %reduce-scatter.8.cloned.1.call-update) | async-done | bytes 131088 | tf_op jit(solution)/shard_map/reduce_scatter | solution.py:88
  189.2 1.5 add_convert_fusion
  (4 shorter events, 0.0 us)
Async XLA Ops:
  7.2 79.3 %copy-start = (bf16[512,1024]{1,0:T(8,128)(2,1)S(1)}, bf16[512,1024]{1,0:T(8,128)(2,1)}, u32[]{:S(2)}) copy-start(bf16[512,1024]{1,0:T(8,128)(2,1)} %param.23) | copy-start | bytes 3145732
  7.2 63.6 %reduce-scatter.4.cloned.1.call-start = ((), (), s32[]{:S(2)}) async-start(), calls=%async_computation.3 | async-start | bytes 655360 | tf_op jit(solution)/shard_map/reduce_scatter | solution.py:74
  30.8 3.6 %copy-start.1 = (f32[64,4,64,64]{3,2,1,0:T(8,128)}, f32[64,4,64,64]{3,2,1,0:T(8,128)S(1)}, u32[]{:S(2)}) copy-start(f32[64,4,64,64]{3,2,1,0:T(8,128)S(1)} %multiply_add_fusion) | copy-start | bytes 12582916
  30.8 12.0 %copy-start.2 = (bf16[256,2048]{1,0:T(8,128)(2,1)S(1)}, bf16[256,2048]{1,0:T(8,128)(2,1)}, u32[]{:S(2)}) copy-start(bf16[256,2048]{1,0:T(8,128)(2,1)} %param.19) | copy-start | bytes 3145732
  30.9 12.0 %copy-start.3 = (bf16[2048,256]{1,0:T(8,128)(2,1)S(1)}, bf16[2048,256]{1,0:T(8,128)(2,1)}, u32[]{:S(2)}) copy-start(bf16[2048,256]{1,0:T(8,128)(2,1)} %param.18) | copy-start | bytes 3145732
  30.9 11.9 %copy-start.4 = (f32[2048]{0:T(1024)S(1)}, f32[2048]{0:T(1024)}, u32[]{:S(2)}) copy-start(f32[2048]{0:T(1024)} %param.20) | copy-start | bytes 24580
  45.3 108.1 %copy-start.5 = (bf16[1024,512]{1,0:T(8,128)(2,1)S(1)}, bf16[1024,512]{1,0:T(8,128)(2,1)}, u32[]{:S(2)}) copy-start(bf16[1024,512]{1,0:T(8,128)(2,1)} %param.24) | copy-start | bytes 3145732
  45.3 79.5 %reduce-scatter.6.cloned.1.call-start = ((), (), s32[]{:S(2)}) async-start(), calls=%async_computation.4 | async-start | bytes 2621440 | tf_op jit(solution)/shard_map/reduce_scatter | solution.py:82
  89.3 64.1 %all-gather.2.cloned.1.call-start = ((), (), s32[]{:S(2)}) async-start(), calls=%async_computation.5 | async-start | bytes 1310720 | tf_op jit(solution)/shard_map/all_gather | solution.py:87
  126.7 62.5 %reduce-scatter.8.cloned.1.call-start = ((), (), s32[]{:S(2)}) async-start(), calls=%async_computation.6 | async-start | bytes 1179648 | tf_op jit(solution)/shard_map/reduce_scatter | solution.py:88
Sparse Core Ops, SparseCore 0:
  45.4 25.3 reduce-scatter.3
  89.4 35.3 reduce-scatter.5
  126.8 26.4 all-gather.1
  156.5 32.6 reduce-scatter.7
where the time goes:
time: 198 us; the launch traced here: 197 us
  waiting for transfers between devices  109 us (55%)
  blocking collectives  34.5 us (17%)
  matrix products  20.3 us (10%)
  between operations  14.6 us (7%)
  other arithmetic  11.8 us (6%)
  local copies, waits for them, and re-layouts  6.66 us (3%)
    reduce_scatter x1, waiting for transfers between devices, on_device(): lax.psum_scatter(jnp.dot(hidden, down_weight, preferred_element_type=jnp....  32.8 us
    all_gather x1, waiting for transfers between devices, on_device(): hidden = lax.all_gather(shared, 'kv', axis=0, tiled=True)  26.6 us
    reduce_scatter x1, waiting for transfers between devices, on_device(): lax.psum_scatter(partial_value, 'kv', scatter_dimension=1, tiled=True)  25.5 us
    reduce_scatter x1, waiting for transfers between devices, on_device(): lax.psum_scatter(raised_part, 'kv', scatter_dimension=0, tiled=True)  24.3 us
    all_gather x1, blocking collectives, on_device(): all_rows = lax.all_gather(after_mixer, 'tp', axis=0, tiled=True)  14.7 us
    all_gather x1, blocking collectives, on_device(): whole_rows = lax.all_gather(tokens, 'kv', axis=1, tiled=True)  10.7 us
    unnamed x1, blocking collectives  9.03 us
    dot_general x1, matrix products, on_device(): jnp.einsum('bhkv,bhk->bhv', new_state, queries, precision=lax.Precision.H...  7.33 us
  transfers between devices with their start and end apart: 4, of which 4 were waited for; matrix products, arithmetic and copies ran while one was open for 1% of the time, Pallas kernels for 0%

commit v1 on v0

v1 whole, which is shorter than its diff:
```python
import functools

import jax
import jax.numpy as jnp
from jax import lax
from jax.experimental import pallas as pl
from jax.experimental.pallas import tpu as pltpu
from jax.sharding import PartitionSpec as P

HEADS = 16
HEAD_DIM = 64
EPS = 1e-06
THETA = 10000.0
CORES = 2
MESH = pl.DeviceIdType.MESH
BF = jnp.bfloat16
F32 = jnp.float32


def dot(a, b):
    return jnp.dot(a, b, preferred_element_type=F32)


def greet(groups):
    barrier = pltpu.get_barrier_semaphore()
    for device in groups:
        pl.semaphore_signal(barrier, inc=1, device_id=device, device_id_type=MESH)
    pl.semaphore_wait(barrier, len(groups))


def send(src, dst, send_sem, recv_sem, device):
    copy = pltpu.make_async_remote_copy(
        src_ref=src,
        dst_ref=dst,
        send_sem=send_sem,
        recv_sem=recv_sem,
        device_id=device,
        device_id_type=MESH,
    )
    copy.start()
    return copy


def head_kernel(
    parts, tok, gain, cosine, sine, wq, wk, wv, wg,
    q_out, k_out, v_out, g_out, rows, normed, own_sem, send_sem, recv_sem,
):
    kv = lax.axis_index("kv")
    peers = [{"kv": lax.rem(kv + d, parts)} for d in range(1, parts)]
    greet(peers)
    copies = [
        send(tok, rows.at[kv], send_sem.at[d], recv_sem.at[d], peer)
        for d, peer in enumerate(peers)
    ]
    own = pltpu.make_async_copy(tok, rows.at[kv], own_sem)
    own.start()
    own.wait()
    for copy in copies:
        copy.wait_recv()
    wide = tok.shape[1]
    total = jnp.zeros((tok.shape[0], 1), F32)
    for k in range(parts):
        x = rows[k].astype(F32)
        total = total + jnp.sum(x * x, axis=1, keepdims=True)
    scale = lax.rsqrt(total / (wide * parts) + EPS)
    for k in range(parts):
        x = rows[k].astype(F32)
        cols = pl.ds(k * wide, wide)
        normed[:, cols] = (x * scale * gain[:, cols]).astype(BF)
    n = normed[...]
    half = HEAD_DIM // 2
    width = wq.shape[1]

    def turn(x):
        lane = lax.broadcasted_iota(jnp.int32, x.shape, 1) % HEAD_DIM
        swapped = jnp.where(
            lane < half, pltpu.roll(x, width - half, 1), pltpu.roll(x, half, 1)
        )
        return x * cosine[...] + swapped * sine[...]

    if width % 128 == 0:
        q_out[...] = turn(dot(n, wq[...]))
        k_out[...] = turn(dot(n, wk[...])) * HEAD_DIM ** (-0.5)
    else:
        def turn_small(x):
            lane = lax.broadcasted_iota(jnp.int32, x.shape, 1) % HEAD_DIM
            swapped = jnp.where(
                lane < half,
                jnp.concatenate([x[:, half:], x[:, :half]], axis=1),
                jnp.concatenate([x[:, width - half:], x[:, : width - half]], axis=1),
            )
            return x * cosine[...] + swapped * sine[...]

        q_out[...] = turn_small(dot(n, wq[...]))
        k_out[...] = turn_small(dot(n, wk[...])) * HEAD_DIM ** (-0.5)
    v_out[...] = dot(n, wv[...])
    g_out[...] = dot(n, wg[...])
    for copy in copies:
        copy.wait_send()


def tail_kernel(
    parts, chips, merged, tok, ow, gain, up, down, out,
    s1, r1, x_all, s2, r2, hid, ps, pr, keep, s3, r3,
    s1_sem, r1_sem, ag_s, ag_r, fw_s, fw_r, s2_sem, r2_sem, hs_sem, hr_sem,
    ps_sem, pr_sem, s3_sem, r3_sem,
):
    kv = lax.axis_index("kv")
    tp = lax.axis_index("tp")
    z = tp // CORES
    c = tp % CORES
    peers = [{"kv": lax.rem(kv + d, parts)} for d in range(1, parts)]
    zpeers = [{"tp": lax.rem(z + d, chips) * CORES + c} for d in range(1, chips)]
    mate = {"tp": z * CORES + 1 - c}
    greet(peers + zpeers + [mate])
    served, wide = tok.shape
    group = CORES * served
    share = group // parts
    ff = up.shape[1]
    pending = []

    copies = []
    for d, peer in enumerate(peers):
        cols = pl.ds(pl.multiple_of(peer["kv"] * wide, wide), wide)
        s1[d] = dot(merged[...], ow[:, cols]).astype(BF)
        copies.append(send(s1.at[d], r1.at[d], s1_sem.at[d], r1_sem.at[d], peer))
    cols = pl.ds(pl.multiple_of(kv * wide, wide), wide)
    acc = dot(merged[...], ow[:, cols])
    for d, copy in enumerate(copies):
        copy.wait_recv()
        acc = acc + r1[d].astype(F32)
    pending += copies
    after = (tok[...].astype(F32) + acc).astype(BF)
    mine, other = pl.ds(0, served), pl.ds(served, served)
    x_all[0, mine] = after
    arrivals = [None] * chips
    for d, peer in enumerate(zpeers, 1):
        arrivals[chips - d] = send(
            x_all.at[0, mine], x_all.at[chips - d, mine],
            ag_s.at[d], ag_r.at[chips - d], peer,
        )
    forwards = [None] * chips
    forwards[0] = send(
        x_all.at[0, mine], x_all.at[0, other], fw_s.at[0], fw_r.at[0], mate
    )
    raised, gathered, paired, final = {}, {}, {}, {}

    def stage_a(s):
        if s:
            arrivals[s].wait_recv()
            forwards[s] = send(
                x_all.at[s, mine], x_all.at[s, other], fw_s.at[s], fw_r.at[s], mate
            )
        forwards[s].wait_recv()
        x = x_all[s].astype(F32)
        square = jnp.broadcast_to(jnp.sum(x * x, axis=1, keepdims=True), (group, 128))
        high = square.astype(BF)
        low = (square - high.astype(F32)).astype(BF)
        lane = lax.broadcasted_iota(jnp.int32, (group, 128), 1)
        tail = jnp.where(lane < 64, high.astype(F32), low.astype(F32))
        r = dot((x * gain[...]).astype(BF), up[...])
        for p in range(parts):
            part = slice(p * share, (p + 1) * share)
            s2[s, p, :, :ff] = r[part].astype(BF)
            s2[s, p, :, ff:] = tail[part].astype(BF)
        raised[s] = [
            send(
                s2.at[s, peer["kv"]], r2.at[s, d],
                s2_sem.at[s, d], r2_sem.at[s, d], peer,
            )
            for d, peer in enumerate(peers)
        ]

    def stage_b(s):
        acc = s2[s, kv].astype(F32)
        for d, copy in enumerate(raised[s]):
            copy.wait_recv()
            acc = acc + r2[s, d].astype(F32)
        total = jnp.sum(acc[:, ff:], axis=1, keepdims=True) * (1.0 / 64)
        factor = lax.rsqrt(total / (wide * parts) + EPS)
        hid[s, kv] = jnp.square(jnp.maximum(acc[:, :ff] * factor, 0.0)).astype(BF)
        gathered[s] = [
            send(
                hid.at[s, kv], hid.at[s, kv],
                hs_sem.at[s, d], hr_sem.at[s, d], peer,
            )
            for d, peer in enumerate(peers)
        ]

    def stage_c(s):
        for copy in gathered[s]:
            copy.wait_recv()
        h = jnp.concatenate([hid[s, p] for p in range(parts)], axis=0)
        lowered = dot(h, down[...])
        ps[s] = lowered[served:].astype(BF)
        paired[s] = send(ps.at[s], pr.at[s], ps_sem.at[s], pr_sem.at[s], mate)
        keep[s] = lowered[:served]

    def stage_d(s):
        paired[s].wait_recv()
        total = keep[s] + pr[s].astype(F32)
        if s == 0:
            keep[0] = total
        else:
            s3[s] = total.astype(BF)
            final[s] = send(
                s3.at[s], r3.at[chips - s],
                s3_sem.at[s], r3_sem.at[chips - s], zpeers[s - 1],
            )

    stages = (stage_a, stage_b, stage_c, stage_d)
    for t in range(chips + 3):
        for lag, stage in enumerate(stages):
            if 0 <= t - lag < chips:
                stage(t - lag)
    acc = keep[0]
    for s in range(1, chips):
        final[s].wait_recv()
        acc = acc + r3[chips - s].astype(F32)
    out[...] = (x_all[0, mine].astype(F32) + acc).astype(BF)
    for copy in pending + arrivals[1:] + forwards:
        copy.wait_send()
    for s in range(chips):
        for copy in raised[s] + gathered[s] + [paired[s]]:
            copy.wait_send()
        if s:
            final[s].wait_send()


VMEM = pl.BlockSpec(memory_space=pltpu.VMEM)
DMA = pltpu.SemaphoreType.DMA


def on_device(
    parts,
    chips,
    tokens,
    lengths,
    query_weight,
    key_weight,
    value_weight,
    gate_weight,
    output_weight,
    mixer_gain,
    group_gain,
    channel_gain,
    up_weight,
    down_weight,
    memory_state,
):
    served, wide = tokens.shape
    width = query_weight.shape[1]
    local_heads = width // HEAD_DIM
    half = HEAD_DIM // 2
    inverse = THETA ** (-jnp.arange(half, dtype=F32) * 2.0 / HEAD_DIM)
    angles = lengths.astype(F32)[:, None] * inverse[None, :]
    cosine, sine = jnp.cos(angles), jnp.sin(angles)
    cosine = jnp.concatenate([cosine, cosine] * local_heads, axis=1)
    sine = jnp.concatenate([-sine, sine] * local_heads, axis=1)
    projected = jax.ShapeDtypeStruct((served, width), F32)
    queries, keys_new, values_new, gating = pl.pallas_call(
        functools.partial(head_kernel, parts),
        out_shape=[projected] * 4,
        in_specs=[VMEM] * 8,
        out_specs=[VMEM] * 4,
        scratch_shapes=[
            pltpu.VMEM((parts, served, wide), BF),
            pltpu.VMEM((served, wide * parts), BF),
            DMA,
            DMA((parts - 1,)),
            DMA((parts - 1,)),
        ],
        compiler_params=pltpu.CompilerParams(collective_id=0, has_side_effects=True),
    )(
        tokens, mixer_gain[None, :], cosine, sine,
        query_weight, key_weight, value_weight, gate_weight,
    )
    queries = queries.reshape(served, local_heads, HEAD_DIM)
    keys_new = keys_new.reshape(served, local_heads, HEAD_DIM)
    values_new = values_new.reshape(served, local_heads, HEAD_DIM)
    head_ids = (lax.axis_index("kv") * local_heads + jnp.arange(local_heads)).astype(F32)
    decays = 1.0 - 2.0 ** (-5.0 - 5.0 * head_ids / (HEADS - 1))
    new_state = (
        decays[None, :, None, None] * memory_state
        + keys_new[:, :, :, None] * values_new[:, :, None, :]
    )
    readout = jnp.einsum("bhkv,bhk->bhv", new_state, queries, precision=lax.Precision.HIGHEST)
    grouped = readout * lax.rsqrt(jnp.mean(readout * readout, axis=-1, keepdims=True) + EPS)
    grouped = grouped * group_gain.reshape(local_heads, HEAD_DIM)
    merged = (grouped.reshape(served, width) * jax.nn.silu(gating)).astype(BF)

    ff = up_weight.shape[1]
    group = CORES * served
    share = group // parts
    pair = (chips, parts - 1)
    mixed = pl.pallas_call(
        functools.partial(tail_kernel, parts, chips),
        out_shape=jax.ShapeDtypeStruct((served, wide), BF),
        in_specs=[VMEM] * 6,
        out_specs=VMEM,
        scratch_shapes=[
            pltpu.VMEM((parts - 1, served, wide), BF),
            pltpu.VMEM((parts - 1, served, wide), BF),
            pltpu.VMEM((chips, group, wide), BF),
            pltpu.VMEM((chips, parts, share, ff + 128), BF),
            pltpu.VMEM((chips, parts - 1, share, ff + 128), BF),
            pltpu.VMEM((chips, parts, share, ff), BF),
            pltpu.VMEM((chips, served, wide), BF),
            pltpu.VMEM((chips, served, wide), BF),
            pltpu.VMEM((chips, served, wide), F32),
            pltpu.VMEM((chips, served, wide), BF),
            pltpu.VMEM((chips, served, wide), BF),
            DMA((parts - 1,)),
            DMA((parts - 1,)),
            DMA((chips,)),
            DMA((chips,)),
            DMA((chips,)),
            DMA((chips,)),
            DMA(pair),
            DMA(pair),
            DMA(pair),
            DMA(pair),
            DMA((chips,)),
            DMA((chips,)),
            DMA((chips,)),
            DMA((chips,)),
        ],
        compiler_params=pltpu.CompilerParams(collective_id=1, has_side_effects=True),
    )(merged, tokens, output_weight, channel_gain[None, :], up_weight, down_weight)
    return (mixed, new_state)


def solution(mesh):
    parts = mesh.shape["kv"]
    chips = mesh.shape["tp"] // CORES
    return jax.shard_map(
        functools.partial(on_device, parts, chips),
        mesh=mesh,
        in_specs=(
            P("tp", "kv"),
            P("tp"),
            P(None, "kv"),
            P(None, "kv"),
            P(None, "kv"),
            P(None, "kv"),
            P("kv", None),
            P(),
            P("kv"),
            P("kv"),
            P("kv", "tp"),
            P("tp", "kv"),
            P("tp", "kv", None, None),
        ),
        out_specs=(P("tp", "kv"), P("tp", "kv", None, None)),
        check_vma=False,
    )
```

time: 198 us -> 83.5 us (0.42)
  waiting for transfers between devices: 109 us -> 0 us
  Pallas kernels: 0 us -> 57.8 us
  blocking collectives: 34.5 us -> 0 us
  between operations: 14.6 us -> 0.72 us
  matrix products: 20.3 us -> 9.52 us
    reduce_scatter x3 -> x0, waiting for transfers between devices: 82.6 us -> none  [the longest x1 32.8 us: on_device(): lax.psum_scatter(jnp.dot(hidden, down_weight, preferred_element_type=jnp....]
    pallas_call x0 -> x2, Pallas kernels: none -> 57.8 us  [the longest x1 46.2 us: on_device(): pl.pallas_call(functools.partial(tail_kernel, parts, chips), out_shape=ja...]
    all_gather x1 -> x0, waiting for transfers between devices: 26.6 us -> none  [on_device(): hidden = lax.all_gather(shared, 'kv', axis=0, tiled=True)]
    all_gather x2 -> x0, blocking collectives: 25.5 us -> none  [the longest x1 14.7 us: on_device(): all_rows = lax.all_gather(after_mixer, 'tp', axis=0, tiled=True)]
    dot_general x6 -> x0, matrix products: 12.9 us -> none  [the longest x3 4.75 us: project(): jnp.dot(normed, weight, preferred_element_type=jnp.float32)]
    unnamed x1 -> x0, blocking collectives: 9.03 us -> none
    convert_element_type x4 -> x2, other arithmetic: 5.07 us -> 1.31 us  [the longest x1 0.66 us: on_device(): angles = lengths.astype(F32)[:, None] * inverse[None, :]]
    unnamed x13 -> x7, local copies, waits for them, and re-layouts: 4.8 us -> 1.49 us
  transfers between devices with their start and end apart: 4 -> 0, of which waited for: 4 -> 0; matrix products, arithmetic and copies ran while one was open for 1% -> 0% of each run, Pallas kernels for 0% -> 0%
where the time goes in v1:
time: 83.5 us; the launch traced here: 83.2 us
  Pallas kernels  57.8 us (69%)
  other arithmetic  9.89 us (12%)
  matrix products  9.52 us (11%)
  local copies, waits for them, and re-layouts  5.22 us (6%)
    pallas_call x1, Pallas kernels, on_device(): pl.pallas_call(functools.partial(tail_kernel, parts, chips), out_shape=ja...  46.2 us
    pallas_call x1, Pallas kernels, on_device(): pl.pallas_call(functools.partial(head_kernel, parts), out_shape=[projecte...  11.6 us
    dot_general x1, matrix products, on_device(): jnp.einsum('bhkv,bhk->bhv', new_state, queries, precision=lax.Precision.H...  9.52 us
    add x1, other arithmetic, on_device(): decays[None, :, None, None] * memory_state  8.08 us
    mul x2, local copies, waits for them, and re-layouts, on_device(): keys_new[:, :, :, None] * values_new[:, :, None, :]  1.9 us

profile of v1, /device:TPU:0, one launch (start us, length us, event | category | flops | bytes accessed | tf_op | source)
XLA Modules:
  0.0 83.2 jit_solution(429542418980821984)
XLA Ops:
  0.6 0.7 convert_element_type.14
  1.3 0.2 multiply_sine_fusion
  1.5 0.8 concatenate.7.sine
  2.3 0.7 concatenate.6.cosine
  3.0 11.6 %shard_map.140 = (f32[64,256]{1,0:T(8,128)}, f32[64,256]{1,0:T(8,128)}, f32[64,256]{1,0:T(8,128)}, f32[64,256]{1,0:T(8,128)}) custom-call(bf16[64,512]{1,0:T(8,128)(2,1)} %tok.3, f32[1,2048]{1,0:T(1,128)} %bitcast.10, f32[64,256]{1,0:T(8,128)} %concatenate.6.cosine, f32[64,256]{1,0:T(8,128)} %concatenate.7.sine, bf16[2048,256]{1,0:T(8,128)(2,1)} %wq.1, ...), custom_call_target="tpu_custom_call" | custom-call | tf_op jit(solution)/shard_map/pallas_call | solution.py:261
  14.7 0.9 %mul.80 = f32[64,4,64]{2,1,0:T(4,128)S(1)} reshape(f32[64,256]{1,0:T(8,128)} %get-tuple-element.6) | data formatting | bytes 131072 | tf_op jit(solution)/shard_map/mul | solution.py:285
  15.6 0.9 %mul.82 = f32[64,4,64]{2,1,0:T(4,128)S(1)} reshape(f32[64,256]{1,0:T(8,128)} %get-tuple-element.7) | data formatting | bytes 131072 | tf_op jit(solution)/shard_map/mul | solution.py:285
  16.6 0.0 copy-start
  16.6 8.1 %multiply_add_fusion = f32[64,4,64,64]{3,2,1,0:T(8,128)} fusion(f32[64,4,64,64]{3,2,1,0:T(8,128)} %param.25, f32[64,4,64]{2,1,0:T(4,128)S(1)} %mul.82, f32[64,4,64]{2,1,0:T(4,128)S(1)} %mul.80, f32[4]{0:T(128)S(1)} %power_subtract_fusion), kind=kLoop, calls=%fused_computation | loop fusion | flops 3145728 | bytes 8519696 | tf_op jit(solution)/shard_map/add | solution.py:284
  24.7 0.0 copy-start.2
  24.7 0.0 copy-start.1
  24.7 0.0 copy-done
  24.7 0.1 reshape.39
  24.8 9.5 %fusion.1 = f32[64,4,1,64]{3,2,1,0:T(1,128)S(1)} fusion(f32[64,4,64,64]{3,2,1,0:T(8,128)} %multiply_add_fusion, f32[64,4,64,1]{2,3,1,0:T(1,128)S(1)} %bitcast.9), kind=kOutput, calls=%fused_computation.10 | convolution fusion | flops 12582912 | bytes 4325376 | tf_op jit(solution)/shard_map/bhkv,bhk->bhv/dot_general | solution.py:287
  34.3 0.1 multiply_reduce_fusion
  34.5 0.0 copy-done.2
  34.5 0.1 mul.88
  34.6 0.1 multiply_multiply_fusion
  34.7 0.1 reshape.38
  34.9 0.0 copy-done.1
  34.9 0.6 multiply_convert_fusion.merged
  35.5 46.2 %shard_map.141 = bf16[64,512]{1,0:T(8,128)(2,1)} custom-call(bf16[64,256]{1,0:T(8,128)(2,1)} %multiply_convert_fusion.merged, bf16[64,512]{1,0:T(8,128)(2,1)} %tok.3, bf16[256,2048]{1,0:T(8,128)(2,1)} %ow.1, f32[1,512]{1,0:T(1,128)} %bitcast.11, bf16[512,1024]{1,0:T(8,128)(2,1)} %up.1, bf16[1024,512]{1,0:T(8,128)(2,1)} %down.1), custom_call_target="tpu_custom_call" | custom-call | tf_op jit(solution)/shard_map/pallas_call | solution.py:296
  81.7 1.5 %copy.22 = bf16[64,512]{1,0:T(8,128)(2,1)} copy(bf16[64,512]{1,0:T(8,128)(2,1)} %shard_map.141) | data formatting | bytes 131072
  (3 shorter events, 0.0 us)
Async XLA Ops:
  16.6 8.1 %copy-start = (f32[64,256]{1,0:T(8,128)S(1)}, f32[64,256]{1,0:T(8,128)}, u32[]{:S(2)}) copy-start(f32[64,256]{1,0:T(8,128)} %get-tuple-element.8) | copy-start | bytes 196612
  24.7 9.8 %copy-start.2 = (f32[256]{0:T(256)S(1)}, f32[256]{0:T(256)}, u32[]{:S(2)}) copy-start(f32[256]{0:T(256)} %param.21) | copy-start | bytes 3076
  24.7 10.2 %copy-start.1 = (f32[64,256]{1,0:T(8,128)S(1)}, f32[64,256]{1,0:T(8,128)}, u32[]{:S(2)}) copy-start(f32[64,256]{1,0:T(8,128)} %get-tuple-element.9) | copy-start | bytes 196612

commit v2 on v1

--- a/solution.py
+++ b/solution.py
@@ -2,6 +2,7 @@
 
 import jax
 import jax.numpy as jnp
+import numpy as np
 from jax import lax
 from jax.experimental import pallas as pl
 from jax.experimental.pallas import tpu as pltpu
@@ -21,11 +22,14 @@
     return jnp.dot(a, b, preferred_element_type=F32)
 
 
-def greet(groups):
+def greet(devices):
     barrier = pltpu.get_barrier_semaphore()
-    for device in groups:
+    for device in devices:
         pl.semaphore_signal(barrier, inc=1, device_id=device, device_id_type=MESH)
-    pl.semaphore_wait(barrier, len(groups))
+
+
+def greeted(devices):
+    pl.semaphore_wait(pltpu.get_barrier_semaphore(), len(devices))
 
 
 def send(src, dst, send_sem, recv_sem, device):
@@ -42,23 +46,43 @@
 
 
 def head_kernel(
-    parts, tok, gain, cosine, sine, wq, wk, wv, wg,
-    q_out, k_out, v_out, g_out, rows, normed, own_sem, send_sem, recv_sem,
+    parts, tok, lengths, inverse, gain, wq, wk, wv, wg,
+    q_out, k_out, v_out, g_out, rows, normed, weights, own_sem, w_sem, send_sem, recv_sem,
 ):
     kv = lax.axis_index("kv")
     peers = [{"kv": lax.rem(kv + d, parts)} for d in range(1, parts)]
     greet(peers)
+    loads = [
+        pltpu.make_async_copy(w, weights.at[i], w_sem.at[i])
+        for i, w in enumerate((wq, wk, wv, wg))
+    ]
+    own = pltpu.make_async_copy(tok, rows.at[kv], own_sem)
+    own.start()
+    for load in loads:
+        load.start()
+    greeted(peers)
     copies = [
         send(tok, rows.at[kv], send_sem.at[d], recv_sem.at[d], peer)
         for d, peer in enumerate(peers)
     ]
-    own = pltpu.make_async_copy(tok, rows.at[kv], own_sem)
-    own.start()
+    served, wide = tok.shape
+    width = q_out.shape[1]
+    half = HEAD_DIM // 2
+    diagonal = lax.broadcasted_iota(jnp.int32, (served, served), 0) == (
+        lax.broadcasted_iota(jnp.int32, (served, served), 1)
+    )
+    position = jnp.sum(
+        jnp.where(diagonal, lengths[...].astype(F32), 0.0), axis=1, keepdims=True
+    )
+    angles = position * inverse[...]
+    first = lax.broadcasted_iota(jnp.int32, (served, width), 1) % HEAD_DIM < half
+    cosine = jnp.cos(angles)
+    sine = jnp.where(first, -jnp.sin(angles), jnp.sin(angles))
+
     own.wait()
     for copy in copies:
         copy.wait_recv()
-    wide = tok.shape[1]
-    total = jnp.zeros((tok.shape[0], 1), F32)
+    total = jnp.zeros((served, 1), F32)
     for k in range(parts):
         x = rows[k].astype(F32)
         total = total + jnp.sum(x * x, axis=1, keepdims=True)
@@ -68,40 +92,62 @@
         cols = pl.ds(k * wide, wide)
         normed[:, cols] = (x * scale * gain[:, cols]).astype(BF)
     n = normed[...]
-    half = HEAD_DIM // 2
-    width = wq.shape[1]
 
     def turn(x):
-        lane = lax.broadcasted_iota(jnp.int32, x.shape, 1) % HEAD_DIM
-        swapped = jnp.where(
-            lane < half, pltpu.roll(x, width - half, 1), pltpu.roll(x, half, 1)
-        )
-        return x * cosine[...] + swapped * sine[...]
-
-    if width % 128 == 0:
-        q_out[...] = turn(dot(n, wq[...]))
-        k_out[...] = turn(dot(n, wk[...])) * HEAD_DIM ** (-0.5)
-    else:
-        def turn_small(x):
-            lane = lax.broadcasted_iota(jnp.int32, x.shape, 1) % HEAD_DIM
-            swapped = jnp.where(
-                lane < half,
-                jnp.concatenate([x[:, half:], x[:, :half]], axis=1),
-                jnp.concatenate([x[:, width - half:], x[:, : width - half]], axis=1),
-            )
-            return x * cosine[...] + swapped * sine[...]
-
-        q_out[...] = turn_small(dot(n, wq[...]))
-        k_out[...] = turn_small(dot(n, wk[...])) * HEAD_DIM ** (-0.5)
-    v_out[...] = dot(n, wv[...])
-    g_out[...] = dot(n, wg[...])
+        back = jnp.concatenate([x[:, half:], x[:, :half]], axis=1)
+        ahead = jnp.concatenate([x[:, width - half :], x[:, : width - half]], axis=1)
+        return x * cosine + jnp.where(first, back, ahead) * sine
+
+    loads[0].wait()
+    q_out[...] = turn(dot(n, weights[0]))
+    loads[1].wait()
+    k_out[...] = turn(dot(n, weights[1])) * HEAD_DIM ** (-0.5)
+    loads[2].wait()
+    v_out[...] = dot(n, weights[2])
+    loads[3].wait()
+    g_out[...] = dot(n, weights[3])
     for copy in copies:
         copy.wait_send()
 
 
+def state_kernel(local, q, k, v, g, gain, state, new_state, merged, readout):
+    step = pl.program_id(0)
+    block = q.shape[0]
+    first = lax.axis_index("kv") * local
+    kt, q_t = k[...].T, q[...].T
+    values = v[...]
+    decays = []
+    for h in range(local):
+        head = jnp.full((1, HEAD_DIM), first + h, jnp.int32).astype(F32)
+        decays.append(1.0 - jnp.exp2(-5.0 - 5.0 * head / (HEADS - 1)))
+    rows = []
+    for b in range(block):
+        pieces = []
+        for h in range(local):
+            cut = slice(h * HEAD_DIM, (h + 1) * HEAD_DIM)
+            new = decays[h] * state[b, h] + kt[cut, b : b + 1] * values[b : b + 1, cut]
+            new_state[b, h] = new
+            pieces.append(jnp.sum(new * q_t[cut, b : b + 1], axis=0, keepdims=True))
+        rows.append(jnp.concatenate(pieces, axis=1))
+    readout[pl.ds(pl.multiple_of(step * block, block), block)] = jnp.concatenate(rows, axis=0)
+
+    @pl.when(step == pl.num_programs(0) - 1)
+    def _():
+        parts = []
+        for h in range(local):
+            x = readout[:, h * HEAD_DIM : (h + 1) * HEAD_DIM]
+            parts.append(
+                x * lax.rsqrt(jnp.mean(x * x, axis=1, keepdims=True) + EPS)
+            )
+        gate = g[...]
+        merged[...] = (
+            jnp.concatenate(parts, axis=1) * gain[...] * (gate * jax.nn.sigmoid(gate))
+        ).astype(BF)
+
+
 def tail_kernel(
-    parts, chips, merged, tok, ow, gain, up, down, out,
-    s1, r1, x_all, s2, r2, hid, ps, pr, keep, s3, r3,
+    parts, chips, merged, tok, ow, gain, up_hbm, down_hbm, out,
+    up, down, w_sem, s1, r1, x_all, s2, r2, hid, ps, pr, keep, s3, r3,
     s1_sem, r1_sem, ag_s, ag_r, fw_s, fw_r, s2_sem, r2_sem, hs_sem, hr_sem,
     ps_sem, pr_sem, s3_sem, r3_sem,
 ):
@@ -113,6 +159,12 @@
     zpeers = [{"tp": lax.rem(z + d, chips) * CORES + c} for d in range(1, chips)]
     mate = {"tp": z * CORES + 1 - c}
     greet(peers + zpeers + [mate])
+    loads = [
+        pltpu.make_async_copy(up_hbm, up, w_sem.at[0]),
+        pltpu.make_async_copy(down_hbm, down, w_sem.at[1]),
+    ]
+    for load in loads:
+        load.start()
     served, wide = tok.shape
     group = CORES * served
     share = group // parts
@@ -123,6 +175,8 @@
     for d, peer in enumerate(peers):
         cols = pl.ds(pl.multiple_of(peer["kv"] * wide, wide), wide)
         s1[d] = dot(merged[...], ow[:, cols]).astype(BF)
+        if d == 0:
+            greeted(peers + zpeers + [mate])
         copies.append(send(s1.at[d], r1.at[d], s1_sem.at[d], r1_sem.at[d], peer))
     cols = pl.ds(pl.multiple_of(kv * wide, wide), wide)
     acc = dot(merged[...], ow[:, cols])
@@ -152,6 +206,8 @@
                 x_all.at[s, mine], x_all.at[s, other], fw_s.at[s], fw_r.at[s], mate
             )
         forwards[s].wait_recv()
+        if s == 0:
+            loads[0].wait()
         x = x_all[s].astype(F32)
         square = jnp.broadcast_to(jnp.sum(x * x, axis=1, keepdims=True), (group, 128))
         high = square.astype(BF)
@@ -190,6 +246,8 @@
     def stage_c(s):
         for copy in gathered[s]:
             copy.wait_recv()
+        if s == 0:
+            loads[1].wait()
         h = jnp.concatenate([hid[s, p] for p in range(parts)], axis=0)
         lowered = dot(h, down[...])
         ps[s] = lowered[served:].astype(BF)
@@ -228,6 +286,7 @@
 
 
 VMEM = pl.BlockSpec(memory_space=pltpu.VMEM)
+ANY = pl.BlockSpec(memory_space=pl.ANY)
 DMA = pltpu.SemaphoreType.DMA
 
 
@@ -251,43 +310,49 @@
     served, wide = tokens.shape
     width = query_weight.shape[1]
     local_heads = width // HEAD_DIM
-    half = HEAD_DIM // 2
-    inverse = THETA ** (-jnp.arange(half, dtype=F32) * 2.0 / HEAD_DIM)
-    angles = lengths.astype(F32)[:, None] * inverse[None, :]
-    cosine, sine = jnp.cos(angles), jnp.sin(angles)
-    cosine = jnp.concatenate([cosine, cosine] * local_heads, axis=1)
-    sine = jnp.concatenate([-sine, sine] * local_heads, axis=1)
+    lane = np.arange(width) % (HEAD_DIM // 2)
+    inverse = (THETA ** (-lane * 2.0 / HEAD_DIM)).astype(np.float32)[None, :]
     projected = jax.ShapeDtypeStruct((served, width), F32)
     queries, keys_new, values_new, gating = pl.pallas_call(
         functools.partial(head_kernel, parts),
         out_shape=[projected] * 4,
-        in_specs=[VMEM] * 8,
+        in_specs=[VMEM] * 4 + [ANY] * 4,
         out_specs=[VMEM] * 4,
         scratch_shapes=[
             pltpu.VMEM((parts, served, wide), BF),
             pltpu.VMEM((served, wide * parts), BF),
+            pltpu.VMEM((4,) + query_weight.shape, BF),
             DMA,
+            DMA((4,)),
             DMA((parts - 1,)),
             DMA((parts - 1,)),
         ],
         compiler_params=pltpu.CompilerParams(collective_id=0, has_side_effects=True),
     )(
-        tokens, mixer_gain[None, :], cosine, sine,
+        tokens, lengths[None, :], jnp.asarray(inverse), mixer_gain[None, :],
         query_weight, key_weight, value_weight, gate_weight,
     )
-    queries = queries.reshape(served, local_heads, HEAD_DIM)
-    keys_new = keys_new.reshape(served, local_heads, HEAD_DIM)
-    values_new = values_new.reshape(served, local_heads, HEAD_DIM)
-    head_ids = (lax.axis_index("kv") * local_heads + jnp.arange(local_heads)).astype(F32)
-    decays = 1.0 - 2.0 ** (-5.0 - 5.0 * head_ids / (HEADS - 1))
-    new_state = (
-        decays[None, :, None, None] * memory_state
-        + keys_new[:, :, :, None] * values_new[:, :, None, :]
-    )
-    readout = jnp.einsum("bhkv,bhk->bhv", new_state, queries, precision=lax.Precision.HIGHEST)
-    grouped = readout * lax.rsqrt(jnp.mean(readout * readout, axis=-1, keepdims=True) + EPS)
-    grouped = grouped * group_gain.reshape(local_heads, HEAD_DIM)
-    merged = (grouped.reshape(served, width) * jax.nn.silu(gating)).astype(BF)
+    block = 8
+    rows = pl.BlockSpec((block, width), lambda i: (i, 0))
+    states = pl.BlockSpec((block,) + memory_state.shape[1:], lambda i: (i, 0, 0, 0))
+    whole = pl.BlockSpec((served, width), lambda i: (0, 0))
+    new_state, merged = pl.pallas_call(
+        functools.partial(state_kernel, local_heads),
+        grid=(served // block,),
+        out_shape=[
+            jax.ShapeDtypeStruct(memory_state.shape, F32),
+            jax.ShapeDtypeStruct((served, width), BF),
+        ],
+        in_specs=[
+            rows, rows, rows, whole,
+            pl.BlockSpec((1, width), lambda i: (0, 0)), states,
+        ],
+        out_specs=[states, whole],
+        scratch_shapes=[pltpu.VMEM((served, width), F32)],
+        cost_estimate=pl.CostEstimate(
+            flops=6 * memory_state.size, bytes_accessed=16 * memory_state.size, transcendentals=0
+        ),
+    )(queries, keys_new, values_new, gating, group_gain[None, :], memory_state)
 
     ff = up_weight.shape[1]
     group = CORES * served
@@ -296,9 +361,12 @@
     mixed = pl.pallas_call(
         functools.partial(tail_kernel, parts, chips),
         out_shape=jax.ShapeDtypeStruct((served, wide), BF),
-        in_specs=[VMEM] * 6,
+        in_specs=[VMEM] * 4 + [ANY] * 2,
         out_specs=VMEM,
         scratch_shapes=[
+            pltpu.VMEM(up_weight.shape, BF),
+            pltpu.VMEM(down_weight.shape, BF),
+            DMA((2,)),
             pltpu.VMEM((parts - 1, served, wide), BF),
             pltpu.VMEM((parts - 1, served, wide), BF),
             pltpu.VMEM((chips, group, wide), BF),

time: 83.5 us -> 79.6 us (0.953)
  Pallas kernels: 57.8 us -> 77.2 us
  other arithmetic: 9.89 us -> 0 us
  matrix products: 9.52 us -> 0 us
  local copies, waits for them, and re-layouts: 5.22 us -> 1.47 us
    pallas_call x0 -> x1, Pallas kernels: none -> 20.4 us  [on_device(): pl.pallas_call(functools.partial(state_kernel, local_heads), grid=(served...]
    dot_general x1 -> x0, matrix products: 9.52 us -> none  [on_device(): jnp.einsum('bhkv,bhk->bhv', new_state, queries, precision=lax.Precision.H...]
    add x1 -> x0, other arithmetic: 8.08 us -> none  [on_device(): decays[None, :, None, None] * memory_state]
    mul x3 -> x0, local copies, waits for them, and re-layouts: 1.98 us -> none  [the longest x2 1.9 us: on_device(): keys_new[:, :, :, None] * values_new[:, :, None, :]]
    concatenate x2 -> x0, local copies, waits for them, and re-layouts: 1.5 us -> none  [the longest x1 0.75 us: on_device(): sine = jnp.concatenate([-sine, sine] * local_heads, axis=1)]
    convert_element_type x2 -> x0, other arithmetic: 1.31 us -> none  [the longest x1 0.66 us: on_device(): angles = lengths.astype(F32)[:, None] * inverse[None, :]]
where the time goes in v2:
time: 79.6 us; the launch traced here: 79.3 us
  Pallas kernels  77.2 us (97%)
  local copies, waits for them, and re-layouts  1.47 us (2%)
    pallas_call x1, Pallas kernels, on_device(): pl.pallas_call(functools.partial(tail_kernel, parts, chips), out_shape=ja...  45.4 us
    pallas_call x1, Pallas kernels, on_device(): pl.pallas_call(functools.partial(state_kernel, local_heads), grid=(served...  20.4 us
    pallas_call x1, Pallas kernels, on_device(): pl.pallas_call(functools.partial(head_kernel, parts), out_shape=[projecte...  11.4 us

profile of v2, /device:TPU:0, one launch (start us, length us, event | category | flops | bytes accessed | tf_op | source)
XLA Modules:
  0.0 79.3 jit_solution(8622275111655009335)
XLA Ops:
  0.6 11.4 %shard_map.149 = (f32[64,256]{1,0:T(8,128)}, f32[64,256]{1,0:T(8,128)}, f32[64,256]{1,0:T(8,128)}, f32[64,256]{1,0:T(8,128)}) custom-call(bf16[64,512]{1,0:T(8,128)(2,1)} %tok.3, s32[1,64]{1,0:T(1,128)} %bitcast.7, f32[1,256]{1,0:T(1,128)} %constant.2.clone.inverse, f32[1,2048]{1,0:T(1,128)} %bitcast.4, bf16[2048,256]{1,0:T(8,128)(2,1)} %wq.1, ...), custom_call_target="tpu_custom_call" | custom-call | tf_op jit(solution)/shard_map/pallas_call | solution.py:316
  12.0 20.4 %shard_map.150 = (f32[64,4,64,64]{3,2,1,0:T(8,128)}, bf16[64,256]{1,0:T(8,128)(2,1)}) custom-call(f32[64,256]{1,0:T(8,128)} %get-tuple-element.8.q, f32[64,256]{1,0:T(8,128)} %get-tuple-element.9.k, f32[64,256]{1,0:T(8,128)} %get-tuple-element.10.v, f32[64,256]{1,0:T(8,128)} %get-tuple-element.11.g, f32[1,256]{1,0:T(1,128)} %bitcast.6, f32[64,4,64,64]{3,2,1,0:T(8,128)} %state.1), custom_call_target="tpu_custom_call" | custom-call | flops 6291456 | bytes 16777216 | tf_op jit(solution)/shard_map/pallas_call | solution.py:339
  32.5 45.4 %shard_map.151 = bf16[64,512]{1,0:T(8,128)(2,1)} custom-call(bf16[64,256]{1,0:T(8,128)(2,1)} %get-tuple-element.12.merged, bf16[64,512]{1,0:T(8,128)(2,1)} %tok.3, bf16[256,2048]{1,0:T(8,128)(2,1)} %ow.1, f32[1,512]{1,0:T(1,128)} %bitcast.5, bf16[512,1024]{1,0:T(8,128)(2,1)} %up_hbm.1, bf16[1024,512]{1,0:T(8,128)(2,1)} %down_hbm.1), custom_call_target="tpu_custom_call" | custom-call | tf_op jit(solution)/shard_map/pallas_call | solution.py:361
  77.9 1.5 %copy.17 = bf16[64,512]{1,0:T(8,128)(2,1)} copy(bf16[64,512]{1,0:T(8,128)(2,1)} %shard_map.151) | data formatting | bytes 131072

commit v3 on v2

--- a/solution.py
+++ b/solution.py
@@ -110,11 +110,21 @@
         copy.wait_send()
 
 
-def state_kernel(local, q, k, v, g, gain, state, new_state, merged, readout):
+def state_kernel(local, q, k, v, g, gain, state, new_state, merged, readout, spread):
     step = pl.program_id(0)
     block = q.shape[0]
     first = lax.axis_index("kv") * local
-    kt, q_t = k[...].T, q[...].T
+    width = q.shape[1]
+    both = jnp.concatenate([k[...], q[...]], axis=1)
+    high = both.astype(BF).astype(F32)
+    rest = both - high
+    middle = rest.astype(BF).astype(F32)
+    pieces = jnp.concatenate([high, middle, rest - middle], axis=0)
+    shape = (3 * block, block * 128)
+    pick = lax.broadcasted_iota(jnp.int32, shape, 0) % block == (
+        lax.broadcasted_iota(jnp.int32, shape, 1) // 128
+    )
+    spread[...] = dot(pieces.T.astype(BF), jnp.where(pick, 1.0, 0.0).astype(BF))
     values = v[...]
     decays = []
     for h in range(local):
@@ -125,9 +135,13 @@
         pieces = []
         for h in range(local):
             cut = slice(h * HEAD_DIM, (h + 1) * HEAD_DIM)
-            new = decays[h] * state[b, h] + kt[cut, b : b + 1] * values[b : b + 1, cut]
+            lanes = slice(b * 128, b * 128 + HEAD_DIM)
+            low = h * HEAD_DIM
+            key = spread[low : low + HEAD_DIM, lanes]
+            query = spread[width + low : width + low + HEAD_DIM, lanes]
+            new = decays[h] * state[b, h] + key * values[b : b + 1, cut]
             new_state[b, h] = new
-            pieces.append(jnp.sum(new * q_t[cut, b : b + 1], axis=0, keepdims=True))
+            pieces.append(jnp.sum(new * query, axis=0, keepdims=True))
         rows.append(jnp.concatenate(pieces, axis=1))
     readout[pl.ds(pl.multiple_of(step * block, block), block)] = jnp.concatenate(rows, axis=0)
 
@@ -156,7 +170,16 @@
     z = tp // CORES
     c = tp % CORES
     peers = [{"kv": lax.rem(kv + d, parts)} for d in range(1, parts)]
-    zpeers = [{"tp": lax.rem(z + d, chips) * CORES + c} for d in range(1, chips)]
+
+    def partner(d):
+        at, bit = z, 1
+        while bit <= d:
+            if d // bit % 2:
+                at = at + bit - 2 * bit * (z // bit % 2)
+            bit *= 2
+        return at
+
+    zpeers = [{"tp": partner(d) * CORES + c} for d in range(1, chips)]
     mate = {"tp": z * CORES + 1 - c}
     greet(peers + zpeers + [mate])
     loads = [
@@ -189,9 +212,8 @@
     x_all[0, mine] = after
     arrivals = [None] * chips
     for d, peer in enumerate(zpeers, 1):
-        arrivals[chips - d] = send(
-            x_all.at[0, mine], x_all.at[chips - d, mine],
-            ag_s.at[d], ag_r.at[chips - d], peer,
+        arrivals[d] = send(
+            x_all.at[0, mine], x_all.at[d, mine], ag_s.at[d], ag_r.at[d], peer
         )
     forwards = [None] * chips
     forwards[0] = send(
@@ -246,7 +268,7 @@
     def stage_c(s):
         for copy in gathered[s]:
             copy.wait_recv()
-        if s == 0:
+        if s == order[0]:
             loads[1].wait()
         h = jnp.concatenate([hid[s, p] for p in range(parts)], axis=0)
         lowered = dot(h, down[...])
@@ -262,19 +284,20 @@
         else:
             s3[s] = total.astype(BF)
             final[s] = send(
-                s3.at[s], r3.at[chips - s],
-                s3_sem.at[s], r3_sem.at[chips - s], zpeers[s - 1],
+                s3.at[s], r3.at[s], s3_sem.at[s], r3_sem.at[s], zpeers[s - 1]
             )
 
-    stages = (stage_a, stage_b, stage_c, stage_d)
-    for t in range(chips + 3):
-        for lag, stage in enumerate(stages):
+    order = [*range(1, chips), 0]
+    for t in range(chips + 4):
+        if t < chips:
+            stage_a(t)
+        for lag, stage in ((2, stage_b), (3, stage_c), (4, stage_d)):
             if 0 <= t - lag < chips:
-                stage(t - lag)
+                stage(order[t - lag])
     acc = keep[0]
     for s in range(1, chips):
         final[s].wait_recv()
-        acc = acc + r3[chips - s].astype(F32)
+        acc = acc + r3[s].astype(F32)
     out[...] = (x_all[0, mine].astype(F32) + acc).astype(BF)
     for copy in pending + arrivals[1:] + forwards:
         copy.wait_send()
@@ -332,7 +355,7 @@
         tokens, lengths[None, :], jnp.asarray(inverse), mixer_gain[None, :],
         query_weight, key_weight, value_weight, gate_weight,
     )
-    block = 8
+    block = 16
     rows = pl.BlockSpec((block, width), lambda i: (i, 0))
     states = pl.BlockSpec((block,) + memory_state.shape[1:], lambda i: (i, 0, 0, 0))
     whole = pl.BlockSpec((served, width), lambda i: (0, 0))
@@ -348,7 +371,10 @@
             pl.BlockSpec((1, width), lambda i: (0, 0)), states,
         ],
         out_specs=[states, whole],
-        scratch_shapes=[pltpu.VMEM((served, width), F32)],
+        scratch_shapes=[
+            pltpu.VMEM((served, width), F32),
+            pltpu.VMEM((2 * width, block * 128), F32),
+        ],
         cost_estimate=pl.CostEstimate(
             flops=6 * memory_state.size, bytes_accessed=16 * memory_state.size, transcendentals=0
         ),

time: 79.6 us -> 66.2 us (0.83)
  Pallas kernels: 77.2 us -> 63.8 us
    pallas_call x1, Pallas kernels: 20.4 us -> 8.91 us  [on_device(): pl.pallas_call(functools.partial(state_kernel, local_heads), grid=(served...]
    pallas_call x1, Pallas kernels: 45.4 us -> 43.4 us  [on_device(): pl.pallas_call(functools.partial(tail_kernel, parts, chips), out_shape=ja...]
where the time goes in v3:
time: 66.2 us; the launch traced here: 65.9 us
  Pallas kernels  63.8 us (96%)
  local copies, waits for them, and re-layouts  1.47 us (2%)
    pallas_call x1, Pallas kernels, on_device(): pl.pallas_call(functools.partial(tail_kernel, parts, chips), out_shape=ja...  43.4 us
    pallas_call x1, Pallas kernels, on_device(): pl.pallas_call(functools.partial(head_kernel, parts), out_shape=[projecte...  11.4 us
    pallas_call x1, Pallas kernels, on_device(): pl.pallas_call(functools.partial(state_kernel, local_heads), grid=(served...  8.91 us
    unnamed x1, local copies, waits for them, and re-layouts  1.47 us

profile of v3, /device:TPU:0, one launch (start us, length us, event | category | flops | bytes accessed | tf_op | source)
XLA Modules:
  0.0 65.9 jit_solution(10737609978611077736)
XLA Ops:
  0.6 11.4 %shard_map.149 = (f32[64,256]{1,0:T(8,128)}, f32[64,256]{1,0:T(8,128)}, f32[64,256]{1,0:T(8,128)}, f32[64,256]{1,0:T(8,128)}) custom-call(bf16[64,512]{1,0:T(8,128)(2,1)} %tok.3, s32[1,64]{1,0:T(1,128)} %bitcast.7, f32[1,256]{1,0:T(1,128)} %constant.2.clone.inverse, f32[1,2048]{1,0:T(1,128)} %bitcast.4, bf16[2048,256]{1,0:T(8,128)(2,1)} %wq.1, ...), custom_call_target="tpu_custom_call" | custom-call | tf_op jit(solution)/shard_map/pallas_call | solution.py:339
  12.0 8.9 %shard_map.150 = (f32[64,4,64,64]{3,2,1,0:T(8,128)}, bf16[64,256]{1,0:T(8,128)(2,1)}) custom-call(f32[64,256]{1,0:T(8,128)} %get-tuple-element.8.q, f32[64,256]{1,0:T(8,128)} %get-tuple-element.9.k, f32[64,256]{1,0:T(8,128)} %get-tuple-element.10.v, f32[64,256]{1,0:T(8,128)} %get-tuple-element.11.g, f32[1,256]{1,0:T(1,128)} %bitcast.6, f32[64,4,64,64]{3,2,1,0:T(8,128)} %state.1), custom_call_target="tpu_custom_call" | custom-call | flops 6291456 | bytes 16777216 | tf_op jit(solution)/shard_map/pallas_call | solution.py:362
  21.0 43.4 %shard_map.151 = bf16[64,512]{1,0:T(8,128)(2,1)} custom-call(bf16[64,256]{1,0:T(8,128)(2,1)} %get-tuple-element.12.merged, bf16[64,512]{1,0:T(8,128)(2,1)} %tok.3, bf16[256,2048]{1,0:T(8,128)(2,1)} %ow.1, f32[1,512]{1,0:T(1,128)} %bitcast.5, bf16[512,1024]{1,0:T(8,128)(2,1)} %up_hbm.1, bf16[1024,512]{1,0:T(8,128)(2,1)} %down_hbm.1), custom_call_target="tpu_custom_call" | custom-call | tf_op jit(solution)/shard_map/pallas_call | solution.py:387
  64.4 1.5 %copy.17 = bf16[64,512]{1,0:T(8,128)(2,1)} copy(bf16[64,512]{1,0:T(8,128)(2,1)} %shard_map.151) | data formatting | bytes 131072
